TPU v7x, 32 devices: a whole 2x2x4 slice. The times are simulated.
32 devices in a mesh: row: 8 (over z, y), col: 4 (over x, core).
Axes of the slice: x: 2, y: 2, z: 4, core: 2. Of those that a mesh axis runs over, the one named last changes fastest.
Arguments:
- tokens: bfloat16 [16384, 2048], P(('row', 'col')), may hold values from -6 to 6
- w_mix: bfloat16 [2048, 512], replicated, may hold values from -0.125 to 0.125
- w_gate: bfloat16 [2048, 2048], replicated, may hold values from -0.125 to 0.125
- gate_bias: float32 [2048], replicated, may hold values from -4 to 4
- w_branch: bfloat16 [512, 2048], replicated, may hold values from -0.25 to 0.25
Outputs:
- mixed: bfloat16 [16384, 2048], P(('row', 'col'))
All inputs are finite; a program needn't handle non-finite values.
Results may differ from a plain program's by a relative error of at most 0.0083.
Values may be sent and summed in bfloat16 or wider, within the bound.
No kernel may reach another device: no remote copies, remote signals or barrier semaphores. Data moves between devices by JAX's collectives and lax.ppermute only.
A program may use at most 64 MiB of HBM per device.

v0:
```python
import math
import jax
import jax.numpy as jnp
from jax import lax
from jax.sharding import PartitionSpec as P

GROUP_DIM = 64
HIGH = lax.Precision.HIGHEST


def phase_table(left, right, period):
    product = left[:, None] * right[None, :] % period
    angle = product.astype(jnp.float32) * (2.0 * math.pi / period)
    return (jnp.cos(angle), jnp.sin(angle))


def group_tables(span):
    index = jnp.arange(span, dtype=jnp.int32)
    inner = index % GROUP_DIM
    cos_c, sin_c = phase_table(inner, inner, GROUP_DIM)
    same = (index[:, None] // GROUP_DIM == index[None, :] // GROUP_DIM).astype(jnp.float32)
    return (cos_c * same, sin_c * same)


def shards(tokens, w_mix, w_gate, gate_bias, w_branch):
    n_dev = lax.axis_size(("row", "col"))
    local_len = tokens.shape[0]
    full_len = local_len * n_dev
    sub_len = local_len // n_dev
    mixed_in = jnp.dot(tokens, w_mix, preferred_element_type=jnp.float32).astype(jnp.bfloat16)
    channels = mixed_in.shape[1]
    span = min(channels, max(GROUP_DIM, 128))
    pieces = lax.all_to_all(
        mixed_in.reshape(1, local_len, channels),
        ("row", "col"),
        split_axis=1,
        concat_axis=0,
        tiled=True,
    )
    values = pieces.astype(jnp.float32)
    dev_iota = jnp.arange(n_dev, dtype=jnp.int32)
    cos_p, sin_p = phase_table(dev_iota, dev_iota, n_dev)
    first_re = jnp.einsum("kn,nmc->kmc", cos_p, values, precision=HIGH)
    first_im = -jnp.einsum("kn,nmc->kmc", sin_p, values, precision=HIGH)
    cos_c, sin_c = group_tables(span)
    shaped = (n_dev, sub_len, channels // span, span)
    part_re = first_re.reshape(shaped)
    part_im = first_im.reshape(shaped)
    chan_re = jnp.einsum("kmgc,cd->kmgd", part_re, cos_c, precision=HIGH) + jnp.einsum(
        "kmgc,cd->kmgd", part_im, sin_c, precision=HIGH
    )
    chan_im = jnp.einsum("kmgc,cd->kmgd", part_im, cos_c, precision=HIGH) - jnp.einsum(
        "kmgc,cd->kmgd", part_re, sin_c, precision=HIGH
    )
    chan_re = chan_re.reshape(n_dev, sub_len, channels)
    chan_im = chan_im.reshape(n_dev, sub_len, channels)
    start = lax.axis_index(("row", "col")) * sub_len
    positions = start + jnp.arange(sub_len, dtype=jnp.int32)
    cos_t, sin_t = phase_table(dev_iota, positions, full_len)
    twist_re = chan_re * cos_t[:, :, None] + chan_im * sin_t[:, :, None]
    twist_im = chan_im * cos_t[:, :, None] - chan_re * sin_t[:, :, None]
    recv_re, recv_im = (
        lax.all_to_all(twist_re, ("row", "col"), split_axis=0, concat_axis=1, tiled=True),
        lax.all_to_all(twist_im, ("row", "col"), split_axis=0, concat_axis=1, tiled=True),
    )
    recv_re = recv_re.reshape(local_len, channels)
    recv_im = recv_im.reshape(local_len, channels)
    len_iota = jnp.arange(local_len, dtype=jnp.int32)
    cos_m, sin_m = phase_table(len_iota, len_iota, local_len)
    real_part = jnp.dot(cos_m, recv_re, precision=HIGH) + jnp.dot(sin_m, recv_im, precision=HIGH)
    real_part = real_part * (1.0 / math.sqrt(full_len * GROUP_DIM))
    freq_rows = real_part.astype(jnp.bfloat16).reshape(local_len, 1, channels)
    spectrum = lax.all_to_all(
        freq_rows, ("row", "col"), split_axis=0, concat_axis=1, tiled=True
    ).reshape(local_len, channels)
    gate = jax.nn.sigmoid(jnp.dot(tokens, w_gate, preferred_element_type=jnp.float32) + gate_bias)
    branch = jnp.dot(spectrum, w_branch, preferred_element_type=jnp.float32)
    return (gate * branch).astype(jnp.bfloat16)


def solution(mesh):
    in_specs = (P(("row", "col"), None), P(), P(), P(), P())
    out_specs = P(("row", "col"), None)
    return jax.shard_map(shards, mesh=mesh, in_specs=in_specs, out_specs=out_specs, check_vma=False)
```

profile of v0, /device:TPU:0, one launch (start us, length us, event | category | flops | bytes accessed | tf_op | source)
XLA Modules:
  0.0 156.2 jit_solution(4183638831278517337)
XLA Ops:
  1.6 2.8 %fusion.5 = bf16[1,512,512]{2,1,0:T(8,128)(2,1)S(1)} fusion(bf16[512,2048]{1,0:T(8,128)(2,1)S(1)} %copy-done, bf16[2048,512]{1,0:T(8,128)(2,1)} %param.6), kind=kOutput, calls=%fused_computation.14 | convolution fusion | flops 1074003968 | bytes 4718592 | tf_op jit(solution)/shard_map/dot_general | solution.py:30
  5.8 4.6 %reduce = bf16[512,512]{1,0:T(8,128)(2,1)} reduce(bf16[512,1,512]{2,1,0:T(2,128)(2,1)S(1)} %bitcast.70, bf16[]{:T(256)} %broadcast.262), dimensions={1}, to_apply=%bitcast.66.reduce_sub_computation | reduce | bytes 1048578
  10.4 2.2 %reshape.199 = bf16[32,2,4096]{2,1,0:T(2,128)(2,1)} reshape(bf16[512,512]{1,0:T(8,128)(2,1)} %reduce) | data formatting | bytes 1048576
  12.7 7.5 %all-to-all-start = ((bf16[32,2,4096]{2,1,0:T(2,128)(2,1)}), bf16[32,2,4096]{2,1,0:T(2,128)(2,1)S(1)}, u32[]{:S(2)}, u32[]{:S(2)}) async-start(bf16[32,2,4096]{2,1,0:T(2,128)(2,1)} %reshape.199), calls=%async_computation | async-start | bytes 1048576 | tf_op jit(solution)/shard_map/all_to_all | solution.py:33
  20.3 15.3 %all-to-all-done = bf16[32,2,4096]{2,1,0:T(2,128)(2,1)S(1)} async-done(((bf16[32,2,4096]{2,1,0:T(2,128)(2,1)}), bf16[32,2,4096]{2,1,0:T(2,128)(2,1)S(1)}, u32[]{:S(2)}, u32[]{:S(2)}) %all-to-all-start) | async-done | bytes 524320 | tf_op jit(solution)/shard_map/all_to_all | solution.py:33
  35.6 1.8 %reshape.200 = bf16[512,1,512]{2,1,0:T(2,128)(2,1)} reshape(bf16[32,2,4096]{2,1,0:T(2,128)(2,1)S(1)} %all-to-all-done) | data formatting | bytes 1048576
  40.5 1.8 %fusion.23 = f32[32,16,4,128]{3,0,2,1:T(8,128)S(1)} fusion(bf16[16,4,128,32]{2,1,0,3:T(4,128)(2,1)} %reshape.198), kind=kOutput, calls=%fused_computation.36 | convolution fusion | flops 100677632 | bytes 1572864 | tf_op jit(solution)/shard_map/kn,nmc->kmc/dot_general | solution.py:43
  42.3 2.9 %convolution_negate_fusion = f32[32,16,512]{2,0,1:T(8,128)} fusion(bf16[32,16,512]{2,1,0:T(8,128)(2,1)} %bitcast.68), kind=kOutput, calls=%fused_computation.4 | convolution fusion | flops 100939776 | bytes 1572864 | tf_op jit(solution)/shard_map/kn,nmc->kmc/dot_general | solution.py:44
  45.1 2.5 %reshape.187 = f32[32,16,4,128]{3,2,0,1:T(4,128)} reshape(f32[32,16,512]{2,0,1:T(8,128)} %convolution_negate_fusion) | data formatting | bytes 2097152 | tf_op jit(solution)/shard_map/reshape | solution.py:48
  47.7 2.0 %fusion.21 = f32[32,16,4,128]{3,1,2,0:T(8,128)S(1)} fusion(f32[32,16,4,128]{3,0,2,1:T(8,128)S(1)} %fusion.23, s32[128]{0:T(128)S(1)} %get-tuple-element.9, s32[128]{0:T(128)S(1)} %get-tuple-element.10), kind=kOutput, calls=%fused_computation.34 | convolution fusion | flops 402915328 | bytes 2098176 | tf_op jit(solution)/shard_map/kmgc,cd->kmgd/dot_general | solution.py:49
  49.7 1.8 %fusion.17 = f32[32,16,4,128]{3,1,2,0:T(8,128)S(1)} fusion(f32[32,16,4,128]{3,2,0,1:T(4,128)S(1)} %copy-done.1, s32[128]{0:T(128)S(1)} %get-tuple-element.9, s32[128]{0:T(128)S(1)} %get-tuple-element.10), kind=kOutput, calls=%fused_computation.30 | convolution fusion | flops 402915328 | bytes 2098176 | tf_op jit(solution)/shard_map/kmgc,cd->kmgd/dot_general | solution.py:52
  51.5 1.8 %fusion.2 = f32[32,4,2,8,128]{4,3,2,1,0:T(8,128)S(1)} fusion(f32[32,16,4,128]{3,1,2,0:T(8,128)S(1)} %fusion.21, f32[32,16,4,128]{3,2,0,1:T(4,128)S(1)} %copy-done.1, s32[128]{0:T(128)S(1)} %get-tuple-element.9, s32[128]{0:T(128)S(1)} %get-tuple-element.10), kind=kOutput, calls=%fused_computation.10 | convolution fusion | flops 403177472 | bytes 3146752 | tf_op jit(solution)/shard_map/kmgc,cd->kmgd/dot_general | solution.py:49
  53.3 2.0 %fusion.1 = f32[32,4,2,8,128]{4,3,2,1,0:T(8,128)S(1)} fusion(f32[32,16,4,128]{3,1,2,0:T(8,128)S(1)} %fusion.17, f32[32,16,4,128]{3,0,2,1:T(8,128)S(1)} %fusion.23, s32[128]{0:T(128)S(1)} %get-tuple-element.9, s32[128]{0:T(128)S(1)} %get-tuple-element.10), kind=kOutput, calls=%fused_computation.8 | convolution fusion | flops 403177472 | bytes 3146752 | tf_op jit(solution)/shard_map/kmgc,cd->kmgd/dot_general | solution.py:52
  56.6 29.1 %all_to_all.45 = f32[32,16,512]{2,1,0:T(8,128)} all-to-all(f32[32,16,512]{2,1,0:T(8,128)S(1)} %get-tuple-element.6), channel_id=1, replica_groups=mesh['row'=8,'col'=4] {'row','col'}, dimensions={0} | all-to-all | bytes 2097152 | tf_op jit(solution)/shard_map/all_to_all | solution.py:63
  85.7 3.8 %all-to-all-start.2 = ((f32[32,16,512]{2,1,0:T(8,128)}), f32[32,16,512]{2,1,0:T(8,128)S(1)}, u32[]{:S(2)}, u32[]{:S(2)}) async-start(f32[32,16,512]{2,1,0:T(8,128)} %get-tuple-element.5), calls=%async_computation.2 | async-start | bytes 2097152 | tf_op jit(solution)/shard_map/all_to_all | solution.py:64
  89.6 8.0 %fusion.12 = f32[512,512]{1,0:T(8,128)} fusion(f32[512,512]{1,0:T(8,128)} %bitcast.73), kind=kOutput, calls=%fused_computation.25 | convolution fusion | flops 1614282752 | bytes 2097152 | tf_op jit(solution)/shard_map/dot_general | solution.py:70
  97.5 18.0 %all-to-all-done.2 = f32[32,16,512]{2,1,0:T(8,128)S(1)} async-done(((f32[32,16,512]{2,1,0:T(8,128)}), f32[32,16,512]{2,1,0:T(8,128)S(1)}, u32[]{:S(2)}, u32[]{:S(2)}) %all-to-all-start.2) | async-done | bytes 1048608 | tf_op jit(solution)/shard_map/all_to_all | solution.py:64
  115.6 7.8 %fusion.4 = bf16[512,1,512]{2,0,1:T(8,128)(2,1)} fusion(f32[512,512]{1,0:T(8,128)} %fusion.12, f32[512,512]{1,0:T(8,128)S(1)} %bitcast.72), kind=kOutput, calls=%fused_computation.13 | convolution fusion | flops 1615069184 | bytes 2621440 | tf_op jit(solution)/shard_map/dot_general | solution.py:70
  123.4 2.1 %reduce.1 = bf16[512,512]{1,0:T(8,128)(2,1)S(1)} reduce(bf16[512,1,512]{2,0,1:T(8,128)(2,1)} %fusion.4, bf16[]{:T(256)} %broadcast.262), dimensions={1}, to_apply=%copy.40.reduce_sub_computation | reduce | bytes 1048578 | tf_op jit(solution)/shard_map/reshape | solution.py:72
  126.6 4.0 %all-to-all-start.3 = ((bf16[32,2,4096]{2,1,0:T(2,128)(2,1)}), bf16[32,2,4096]{2,1,0:T(2,128)(2,1)}, u32[]{:S(2)}, u32[]{:S(2)}) async-start(bf16[32,2,4096]{2,1,0:T(2,128)(2,1)} %reshape.201), calls=%async_computation.3 | async-start | bytes 1048576 | tf_op jit(solution)/shard_map/all_to_all | solution.py:73
  130.6 9.4 %fusion.109 = f32[512,2048]{1,0:T(8,128)} fusion(bf16[512,2048]{1,0:T(8,128)(2,1)S(1)} %copy-done, bf16[2048,2048]{1,0:T(8,128)(2,1)} %param.7), kind=kOutput, calls=%fused_computation.130 | convolution fusion | flops 4294967296 | bytes 14680064 | tf_op jit(solution)/shard_map/dot_general | solution.py:76
  140.0 6.0 %all-to-all-done.3 = bf16[32,2,4096]{2,1,0:T(2,128)(2,1)} async-done(((bf16[32,2,4096]{2,1,0:T(2,128)(2,1)}), bf16[32,2,4096]{2,1,0:T(2,128)(2,1)}, u32[]{:S(2)}, u32[]{:S(2)}) %all-to-all-start.3) | async-done | bytes 524320 | tf_op jit(solution)/shard_map/all_to_all | solution.py:73
  146.0 3.6 %reshape.202 = bf16[512,1,512]{2,1,0:T(2,128)(2,1)S(1)} reshape(bf16[32,2,4096]{2,1,0:T(2,128)(2,1)} %all-to-all-done.3) | data formatting | bytes 1048576
  151.2 5.0 %multiply_convert_fusion = bf16[512,2048]{1,0:T(8,128)(2,1)} fusion(f32[512,2048]{1,0:T(8,128)} %fusion.109, bf16[512,512]{1,0:T(8,128)(2,1)S(1)} %bitcast.74, bf16[512,2048]{1,0:T(8,128)(2,1)S(1)} %copy-done.3, f32[2048]{0:T(1024)S(1)} %copy-done.4), kind=kOutput, calls=%fused_computation | convolution fusion | flops 1080033280 | bytes 8921088 | tf_op jit(solution)/shard_map/dot_general | solution.py:77
  (21 shorter events, 10.2 us)
Async XLA Ops:
  0.0 1.6 %copy-start = (bf16[512,2048]{1,0:T(8,128)(2,1)S(1)}, bf16[512,2048]{1,0:T(8,128)(2,1)}, u32[]{:S(2)}) copy-start(bf16[512,2048]{1,0:T(8,128)(2,1)} %param.5) | copy-start | bytes 6291460
  12.7 22.9 %all-to-all-start = ((bf16[32,2,4096]{2,1,0:T(2,128)(2,1)}), bf16[32,2,4096]{2,1,0:T(2,128)(2,1)S(1)}, u32[]{:S(2)}, u32[]{:S(2)}) async-start(bf16[32,2,4096]{2,1,0:T(2,128)(2,1)} %reshape.199), calls=%async_computation | async-start | bytes 1048576 | tf_op jit(solution)/shard_map/all_to_all | solution.py:33
  38.7 0.8 copy-start.2
  47.7 2.0 %copy-start.1 = (f32[32,16,4,128]{3,2,0,1:T(4,128)S(1)}, f32[32,16,4,128]{3,2,0,1:T(4,128)}, u32[]{:S(2)}) copy-start(f32[32,16,4,128]{3,2,0,1:T(4,128)} %reshape.187) | copy-start | bytes 3145732
  85.7 29.8 %all-to-all-start.2 = ((f32[32,16,512]{2,1,0:T(8,128)}), f32[32,16,512]{2,1,0:T(8,128)S(1)}, u32[]{:S(2)}, u32[]{:S(2)}) async-start(f32[32,16,512]{2,1,0:T(8,128)} %get-tuple-element.5), calls=%async_computation.2 | async-start | bytes 2097152 | tf_op jit(solution)/shard_map/all_to_all | solution.py:64
  126.6 19.3 %all-to-all-start.3 = ((bf16[32,2,4096]{2,1,0:T(2,128)(2,1)}), bf16[32,2,4096]{2,1,0:T(2,128)(2,1)}, u32[]{:S(2)}, u32[]{:S(2)}) async-start(bf16[32,2,4096]{2,1,0:T(2,128)(2,1)} %reshape.201), calls=%async_computation.3 | async-start | bytes 1048576 | tf_op jit(solution)/shard_map/all_to_all | solution.py:73
  140.0 10.0 %copy-start.4 = (f32[2048]{0:T(1024)S(1)}, f32[2048]{0:T(1024)}, u32[]{:S(2)}) copy-start(f32[2048]{0:T(1024)} %param.8) | copy-start | bytes 24580
  149.6 1.6 %copy-start.3 = (bf16[512,2048]{1,0:T(8,128)(2,1)S(1)}, bf16[512,2048]{1,0:T(8,128)(2,1)}, u32[]{:S(2)}) copy-start(bf16[512,2048]{1,0:T(8,128)(2,1)} %param.9) | copy-start | bytes 6291460
where the time goes:
time: 157 us; the launch traced here: 156 us
  matrix products  45.3 us (29%)
  waiting for transfers between devices  39.3 us (25%)
  blocking collectives  29.1 us (19%)
  local copies, waits for them, and re-layouts  18.9 us (12%)
  starting transfers between devices  15.4 us (10%)
  other arithmetic  8.03 us (5%)
    all_to_all x1, blocking collectives, shards(): lax.all_to_all(twist_re, ('row', 'col'), split_axis=0, concat_axis=1, til...  29.1 us
    all_to_all x1, waiting for transfers between devices, shards(): lax.all_to_all(twist_im, ('row', 'col'), split_axis=0, concat_axis=1, til...  18 us
    all_to_all x1, waiting for transfers between devices, shards(): lax.all_to_all(mixed_in.reshape(1, local_len, channels), ('row', 'col'),...  15.3 us
    unnamed x17, local copies, waits for them, and re-layouts  14.4 us
    dot_general x1, matrix products, shards(): jnp.dot(tokens, w_gate, preferred_element_type=jnp.float32) + gate_bias  9.37 us
    dot_general x1, matrix products, shards(): jnp.dot(cos_m, recv_re, precision=HIGH)  7.95 us
    dot_general x1, matrix products, shards(): jnp.dot(sin_m, recv_im, precision=HIGH)  7.84 us
    all_to_all x1, starting transfers between devices, shards(): lax.all_to_all(mixed_in.reshape(1, local_len, channels), ('row', 'col'),...  7.51 us
  transfers between devices with their start and end apart: 3, of which 3 were waited for; matrix products, arithmetic and copies ran while one was open for 11% of the time, Pallas kernels for 0%

commit v1 on v0

--- a/solution.py
+++ b/solution.py
@@ -6,6 +6,13 @@
 
 GROUP_DIM = 64
 HIGH = lax.Precision.HIGHEST
+
+
+def exchange_blocks(x, name, split, join):
+    count = lax.axis_size(name)
+    blocks = jnp.stack(jnp.split(x, count, axis=split), axis=0)
+    blocks = lax.all_to_all(blocks, name, split_axis=0, concat_axis=0)
+    return jnp.concatenate(blocks, axis=join)
 
 
 def phase_table(left, right, period):
@@ -70,9 +77,7 @@
     real_part = jnp.dot(cos_m, recv_re, precision=HIGH) + jnp.dot(sin_m, recv_im, precision=HIGH)
     real_part = real_part * (1.0 / math.sqrt(full_len * GROUP_DIM))
     freq_rows = real_part.astype(jnp.bfloat16).reshape(local_len, 1, channels)
-    spectrum = lax.all_to_all(
-        freq_rows, ("row", "col"), split_axis=0, concat_axis=1, tiled=True
-    ).reshape(local_len, channels)
+    spectrum = exchange_blocks(freq_rows, ("row", "col"), 0, 1).reshape(local_len, channels)
     gate = jax.nn.sigmoid(jnp.dot(tokens, w_gate, preferred_element_type=jnp.float32) + gate_bias)
     branch = jnp.dot(spectrum, w_branch, preferred_element_type=jnp.float32)
     return (gate * branch).astype(jnp.bfloat16)

time: 157 us -> 168 us (1.070)
  local copies, waits for them, and re-layouts: 18.9 us -> 32.2 us
  other arithmetic: 8.03 us -> 5.97 us
    unnamed x17 -> x43, local copies, waits for them, and re-layouts: 14.4 us -> 27.1 us
    reshape x1 -> x0, other arithmetic: 2.06 us -> none  [shards(): freq_rows = real_part.astype(jnp.bfloat16).reshape(local_len, 1, channels)]
  transfers between devices with their start and end apart: 3 -> 3, of which waited for: 3 -> 3; matrix products, arithmetic and copies ran while one was open for 11% -> 10% of each run, Pallas kernels for 0% -> 0%
where the time goes in v1:
time: 168 us; the launch traced here: 167 us
  matrix products  45.3 us (27%)
  waiting for transfers between devices  39.3 us (23%)
  local copies, waits for them, and re-layouts  32.2 us (19%)
  blocking collectives  29.1 us (17%)
  starting transfers between devices  15.2 us (9%)
  other arithmetic  5.97 us (4%)
    all_to_all x1, blocking collectives, shards(): lax.all_to_all(twist_re, ('row', 'col'), split_axis=0, concat_axis=1, til...  29.1 us
    unnamed x43, local copies, waits for them, and re-layouts  27.1 us
    all_to_all x1, waiting for transfers between devices, shards(): lax.all_to_all(twist_im, ('row', 'col'), split_axis=0, concat_axis=1, til...  18 us
    all_to_all x1, waiting for transfers between devices, shards(): lax.all_to_all(mixed_in.reshape(1, local_len, channels), ('row', 'col'),...  15.3 us
    dot_general x1, matrix products, shards(): jnp.dot(tokens, w_gate, preferred_element_type=jnp.float32) + gate_bias  9.39 us
    dot_general x1, matrix products, shards(): jnp.dot(cos_m, recv_re, precision=HIGH)  7.94 us
    all_to_all x1, starting transfers between devices, shards(): lax.all_to_all(mixed_in.reshape(1, local_len, channels), ('row', 'col'),...  7.51 us
    dot_general x1, matrix products, shards(): jnp.dot(sin_m, recv_im, precision=HIGH)  7.14 us
  transfers between devices with their start and end apart: 3, of which 3 were waited for; matrix products, arithmetic and copies ran while one was open for 10% of the time, Pallas kernels for 0%

profile of v1, /device:TPU:0, one launch (start us, length us, event | category | flops | bytes accessed | tf_op | source)
XLA Modules:
  0.0 167.3 jit_solution(13768814944732269448)
XLA Ops:
  0.0 1.6 copy-done
  1.6 2.8 %fusion.4 = bf16[1,512,512]{2,1,0:T(8,128)(2,1)S(1)} fusion(bf16[512,2048]{1,0:T(8,128)(2,1)S(1)} %copy-done, bf16[2048,512]{1,0:T(8,128)(2,1)} %param.6), kind=kOutput, calls=%fused_computation.13 | convolution fusion | flops 1074003968 | bytes 4718592 | tf_op jit(solution)/shard_map/dot_general | solution.py:37
  5.8 4.6 %reduce = bf16[512,512]{1,0:T(8,128)(2,1)} reduce(bf16[512,1,512]{2,1,0:T(2,128)(2,1)S(1)} %bitcast.194, bf16[]{:T(256)} %broadcast.262), dimensions={1}, to_apply=%bitcast.190.reduce_sub_computation | reduce | bytes 1048578
  10.4 2.2 %reshape.259 = bf16[32,2,4096]{2,1,0:T(2,128)(2,1)} reshape(bf16[512,512]{1,0:T(8,128)(2,1)} %reduce) | data formatting | bytes 1048576
  12.6 7.5 %all-to-all-start = ((bf16[32,2,4096]{2,1,0:T(2,128)(2,1)}), bf16[32,2,4096]{2,1,0:T(2,128)(2,1)S(1)}, u32[]{:S(2)}, u32[]{:S(2)}) async-start(bf16[32,2,4096]{2,1,0:T(2,128)(2,1)} %reshape.259), calls=%async_computation | async-start | bytes 1048576 | tf_op jit(solution)/shard_map/all_to_all | solution.py:40
  20.2 15.3 %all-to-all-done = bf16[32,2,4096]{2,1,0:T(2,128)(2,1)S(1)} async-done(((bf16[32,2,4096]{2,1,0:T(2,128)(2,1)}), bf16[32,2,4096]{2,1,0:T(2,128)(2,1)S(1)}, u32[]{:S(2)}, u32[]{:S(2)}) %all-to-all-start) | async-done | bytes 524320 | tf_op jit(solution)/shard_map/all_to_all | solution.py:40
  35.6 1.8 %reshape.260 = bf16[512,1,512]{2,1,0:T(2,128)(2,1)} reshape(bf16[32,2,4096]{2,1,0:T(2,128)(2,1)S(1)} %all-to-all-done) | data formatting | bytes 1048576
  37.3 1.3 copy.46
  40.4 1.8 %fusion.22 = f32[32,16,4,128]{3,0,2,1:T(8,128)S(1)} fusion(bf16[16,4,128,32]{2,1,0,3:T(4,128)(2,1)} %reshape.258), kind=kOutput, calls=%fused_computation.35 | convolution fusion | flops 100677632 | bytes 1572864 | tf_op jit(solution)/shard_map/kn,nmc->kmc/dot_general | solution.py:50
  42.2 2.9 %convolution_negate_fusion = f32[32,16,512]{2,0,1:T(8,128)} fusion(bf16[32,16,512]{2,1,0:T(8,128)(2,1)} %bitcast.192), kind=kOutput, calls=%fused_computation.4 | convolution fusion | flops 100939776 | bytes 1572864 | tf_op jit(solution)/shard_map/kn,nmc->kmc/dot_general | solution.py:51
  45.1 2.5 %reshape.248 = f32[32,16,4,128]{3,2,0,1:T(4,128)} reshape(f32[32,16,512]{2,0,1:T(8,128)} %convolution_negate_fusion) | data formatting | bytes 2097152 | tf_op jit(solution)/shard_map/reshape | solution.py:55
  47.6 2.0 %fusion.20 = f32[32,16,4,128]{3,1,2,0:T(8,128)S(1)} fusion(f32[32,16,4,128]{3,0,2,1:T(8,128)S(1)} %fusion.22, s32[128]{0:T(128)S(1)} %get-tuple-element.9, s32[128]{0:T(128)S(1)} %get-tuple-element.10), kind=kOutput, calls=%fused_computation.33 | convolution fusion | flops 402915328 | bytes 2098176 | tf_op jit(solution)/shard_map/kmgc,cd->kmgd/dot_general | solution.py:56
  49.6 1.8 %fusion.16 = f32[32,16,4,128]{3,1,2,0:T(8,128)S(1)} fusion(f32[32,16,4,128]{3,2,0,1:T(4,128)S(1)} %copy-done.1, s32[128]{0:T(128)S(1)} %get-tuple-element.9, s32[128]{0:T(128)S(1)} %get-tuple-element.10), kind=kOutput, calls=%fused_computation.29 | convolution fusion | flops 402915328 | bytes 2098176 | tf_op jit(solution)/shard_map/kmgc,cd->kmgd/dot_general | solution.py:59
  51.4 1.8 %fusion.2 = f32[32,4,2,8,128]{4,3,2,1,0:T(8,128)S(1)} fusion(f32[32,16,4,128]{3,1,2,0:T(8,128)S(1)} %fusion.20, f32[32,16,4,128]{3,2,0,1:T(4,128)S(1)} %copy-done.1, s32[128]{0:T(128)S(1)} %get-tuple-element.9, s32[128]{0:T(128)S(1)} %get-tuple-element.10), kind=kOutput, calls=%fused_computation.10 | convolution fusion | flops 403177472 | bytes 3146752 | tf_op jit(solution)/shard_map/kmgc,cd->kmgd/dot_general | solution.py:56
  53.3 2.0 %fusion.1 = f32[32,4,2,8,128]{4,3,2,1,0:T(8,128)S(1)} fusion(f32[32,16,4,128]{3,1,2,0:T(8,128)S(1)} %fusion.16, f32[32,16,4,128]{3,0,2,1:T(8,128)S(1)} %fusion.22, s32[128]{0:T(128)S(1)} %get-tuple-element.9, s32[128]{0:T(128)S(1)} %get-tuple-element.10), kind=kOutput, calls=%fused_computation.8 | convolution fusion | flops 403177472 | bytes 3146752 | tf_op jit(solution)/shard_map/kmgc,cd->kmgd/dot_general | solution.py:59
  56.6 29.1 %all_to_all.35 = f32[32,16,512]{2,1,0:T(8,128)} all-to-all(f32[32,16,512]{2,1,0:T(8,128)S(1)} %get-tuple-element.6), channel_id=1, replica_groups=mesh['row'=8,'col'=4] {'row','col'}, dimensions={0} | all-to-all | bytes 2097152 | tf_op jit(solution)/shard_map/all_to_all | solution.py:70
  85.7 3.8 %all-to-all-start.2 = ((f32[32,16,512]{2,1,0:T(8,128)}), f32[32,16,512]{2,1,0:T(8,128)S(1)}, u32[]{:S(2)}, u32[]{:S(2)}) async-start(f32[32,16,512]{2,1,0:T(8,128)} %get-tuple-element.5), calls=%async_computation.2 | async-start | bytes 2097152 | tf_op jit(solution)/shard_map/all_to_all | solution.py:71
  89.5 7.9 %fusion.11 = f32[512,512]{1,0:T(8,128)} fusion(f32[512,512]{1,0:T(8,128)} %bitcast.197), kind=kOutput, calls=%fused_computation.24 | convolution fusion | flops 1614282752 | bytes 2097152 | tf_op jit(solution)/shard_map/dot_general | solution.py:77
  97.4 18.0 %all-to-all-done.2 = f32[32,16,512]{2,1,0:T(8,128)S(1)} async-done(((f32[32,16,512]{2,1,0:T(8,128)}), f32[32,16,512]{2,1,0:T(8,128)S(1)}, u32[]{:S(2)}, u32[]{:S(2)}) %all-to-all-start.2) | async-done | bytes 1048608 | tf_op jit(solution)/shard_map/all_to_all | solution.py:71
  115.5 7.1 %fusion.3 = bf16[512,512]{1,0:T(8,128)(2,1)S(1)} fusion(f32[512,512]{1,0:T(8,128)} %fusion.11, f32[512,512]{1,0:T(8,128)S(1)} %bitcast.196), kind=kOutput, calls=%fused_computation.12 | convolution fusion | flops 1615069184 | bytes 2621440 | tf_op jit(solution)/shard_map/dot_general | solution.py:77
  142.1 3.9 %all-to-all-start.3 = ((bf16[32,16,1,512]{3,1,2,0:T(8,128)(2,1)}), bf16[32,16,1,512]{3,1,2,0:T(8,128)(2,1)S(1)}, u32[]{:S(2)}, u32[]{:S(2)}) async-start(bf16[32,16,1,512]{3,1,2,0:T(8,128)(2,1)} %constant_dynamic-update-slice_fusion), calls=%async_computation.3 | async-start | bytes 1048576 | tf_op jit(solution)/shard_map/all_to_all | solution.py:14
  146.0 9.4 %fusion.108 = f32[512,2048]{1,0:T(8,128)} fusion(bf16[512,2048]{1,0:T(8,128)(2,1)S(1)} %copy-done, bf16[2048,2048]{1,0:T(8,128)(2,1)} %param.7), kind=kOutput, calls=%fused_computation.193 | convolution fusion | flops 4294967296 | bytes 14680064 | tf_op jit(solution)/shard_map/dot_general | solution.py:81
  155.4 5.9 %all-to-all-done.3 = bf16[32,16,1,512]{3,1,2,0:T(8,128)(2,1)S(1)} async-done(((bf16[32,16,1,512]{3,1,2,0:T(8,128)(2,1)}), bf16[32,16,1,512]{3,1,2,0:T(8,128)(2,1)S(1)}, u32[]{:S(2)}, u32[]{:S(2)}) %all-to-all-start.3) | async-done | bytes 524320 | tf_op jit(solution)/shard_map/all_to_all | solution.py:14
  161.6 5.6 %multiply_convert_fusion = bf16[512,2048]{1,0:T(8,128)(2,1)} fusion(f32[512,2048]{1,0:T(8,128)} %fusion.108, bf16[512,512]{1,0:T(8,128)(2,1)S(1)} %bitcast.198, bf16[512,2048]{1,0:T(8,128)(2,1)} %param.9, f32[2048]{0:T(1024)S(1)} %copy-done.3), kind=kOutput, calls=%fused_computation | convolution fusion | flops 1080033280 | bytes 8921088 | tf_op jit(solution)/shard_map/dot_general | solution.py:82
  (47 shorter events, 24.1 us)
Async XLA Ops:
  0.0 1.6 copy-start
  12.6 22.9 %all-to-all-start = ((bf16[32,2,4096]{2,1,0:T(2,128)(2,1)}), bf16[32,2,4096]{2,1,0:T(2,128)(2,1)S(1)}, u32[]{:S(2)}, u32[]{:S(2)}) async-start(bf16[32,2,4096]{2,1,0:T(2,128)(2,1)} %reshape.259), calls=%async_computation | async-start | bytes 1048576 | tf_op jit(solution)/shard_map/all_to_all | solution.py:40
  38.7 0.8 copy-start.2
  47.6 2.0 %copy-start.1 = (f32[32,16,4,128]{3,2,0,1:T(4,128)S(1)}, f32[32,16,4,128]{3,2,0,1:T(4,128)}, u32[]{:S(2)}) copy-start(f32[32,16,4,128]{3,2,0,1:T(4,128)} %reshape.248) | copy-start | bytes 3145732
  85.7 29.8 %all-to-all-start.2 = ((f32[32,16,512]{2,1,0:T(8,128)}), f32[32,16,512]{2,1,0:T(8,128)S(1)}, u32[]{:S(2)}, u32[]{:S(2)}) async-start(f32[32,16,512]{2,1,0:T(8,128)} %get-tuple-element.5), calls=%async_computation.2 | async-start | bytes 2097152 | tf_op jit(solution)/shard_map/all_to_all | solution.py:71
  142.1 19.2 %all-to-all-start.3 = ((bf16[32,16,1,512]{3,1,2,0:T(8,128)(2,1)}), bf16[32,16,1,512]{3,1,2,0:T(8,128)(2,1)S(1)}, u32[]{:S(2)}, u32[]{:S(2)}) async-start(bf16[32,16,1,512]{3,1,2,0:T(8,128)(2,1)} %constant_dynamic-update-slice_fusion), calls=%async_computation.3 | async-start | bytes 1048576 | tf_op jit(solution)/shard_map/all_to_all | solution.py:14
  146.0 15.7 %copy-start.3 = (f32[2048]{0:T(1024)S(1)}, f32[2048]{0:T(1024)}, u32[]{:S(2)}) copy-start(f32[2048]{0:T(1024)} %param.8) | copy-start | bytes 24580
